TPU v7x, 32 devices: a whole 2x2x4 slice. The times are simulated.
32 devices in a mesh: sp: 16 (over z, y, x), tp: 2 (over core).
Axes of the slice: x: 2, y: 2, z: 4, core: 2. Of those that a mesh axis runs over, the one named last changes fastest.
Arguments:
- stream_in: bfloat16 [4096, 2048], P('sp'), may hold values from -6 to 6
- norm_gain: float32 [2, 2048], replicated, may hold values from 0.1 to 1.9
- value_weight: bfloat16 [2, 2048, 2048], P(None, 'sp', 'tp'), may hold values from -0.125 to 0.125
- gate_weight: bfloat16 [2, 2048, 2048], P(None, 'sp', 'tp'), may hold values from -0.125 to 0.125
- conv_taps: float32 [2, 31, 2048], P(None, None, 'tp'), may hold values from -5 to 5
- channel_gain: float32 [2, 2048], P(None, 'tp'), may hold values from 0.1 to 1.9
- out_weight: bfloat16 [2, 2048, 2048], P(None, 'tp', 'sp'), may hold values from -0.125 to 0.125
Outputs:
- stream_out: bfloat16 [4096, 2048], P('sp')
All inputs are finite; a program needn't handle non-finite values.
Results may differ from a plain program's by a relative error of at most 0.015.
Values may be sent and summed in bfloat16 or wider, within the bound.
A program may use at most 64 MiB of HBM per device.

v0:
```python
import jax
import jax.numpy as jnp
from jax import lax
from jax.sharding import PartitionSpec as P

LAYERS = 2
epsilon = 1e-05


def passed_along(value, axis, steps):
    count = lax.axis_size(axis)
    leading, last = (max(0, -steps), min(count, count - steps))
    return lax.ppermute(value, axis, [(source, source + steps) for source in range(leading, last)])


def body(stream_in, norm_gain, value_weight, gate_weight, conv_taps, channel_gain, out_weight):
    stream = stream_in
    tok_rows = stream_in.shape[0]
    width = stream_in.shape[1]
    kernel = conv_taps.shape[1]
    local_cols = value_weight.shape[2]
    for layer in range(LAYERS):
        wide = stream.astype(jnp.float32)
        normed = (
            wide
            * lax.rsqrt(jnp.mean(wide * wide, axis=1, keepdims=True) + epsilon)
            * norm_gain[layer]
        ).astype(jnp.bfloat16)
        value = jnp.dot(
            normed,
            lax.all_gather(value_weight[layer], "sp", axis=0, tiled=True),
            preferred_element_type=jnp.float32,
        )
        gate = jnp.dot(
            normed,
            lax.all_gather(gate_weight[layer], "sp", axis=0, tiled=True),
            preferred_element_type=jnp.float32,
        )
        gated = (value * jax.nn.sigmoid(gate)).astype(jnp.bfloat16)
        earlier = passed_along(gated[tok_rows - (kernel - 1) :], "sp", 1)
        padded = jnp.concatenate([earlier, gated], axis=0).astype(jnp.float32)
        taps = conv_taps[layer]
        filtered = jnp.zeros((tok_rows, local_cols), jnp.float32)
        for tap in range(kernel):
            filtered = filtered + taps[tap] * padded[tap : tap + tok_rows]
        sum_first, sum_second = lax.psum(
            (jnp.sum(filtered, axis=1), jnp.sum(filtered * filtered, axis=1)), "tp"
        )
        mean_value = (sum_first / width)[:, None]
        variance = (sum_second / width)[:, None] - mean_value * mean_value
        activated = jax.nn.silu(
            (filtered - mean_value) * lax.rsqrt(variance + epsilon) * channel_gain[layer]
        ).astype(jnp.bfloat16)
        whole_out = lax.all_gather(out_weight[layer], "sp", axis=1, tiled=True)
        terms = jnp.dot(activated, whole_out, preferred_element_type=jnp.float32)
        summed = lax.psum(terms.astype(jnp.bfloat16), "tp").astype(jnp.float32)
        stream = (wide + summed).astype(jnp.bfloat16)
    return stream


def solution(mesh):
    return jax.shard_map(
        body,
        mesh=mesh,
        in_specs=(
            P("sp", None),
            P(),
            P(None, "sp", "tp"),
            P(None, "sp", "tp"),
            P(None, None, "tp"),
            P(None, "tp"),
            P(None, "tp", "sp"),
        ),
        out_specs=P("sp", None),
        check_vma=False,
    )
```

profile of v0, /device:TPU:0, one launch (start us, length us, event | category | flops | bytes accessed | tf_op | source)
XLA Modules:
  0.0 556.1 jit_solution(6253315192449355150)
XLA Ops:
  6.5 2.0 fusion.142
  8.6 1.9 fusion.141
  12.0 76.4 %all-gather.15.cloned.1.call-done = bf16[1,2048,1024]{2,1,0:T(8,128)(2,1)} async-done(((bf16[1,128,1024]{2,1,0:T(8,128)(2,1)}), bf16[1,2048,1024]{2,1,0:T(8,128)(2,1)}) %all-gather.15.cloned.1.call-update) | async-done | bytes 4194320 | tf_op jit(solution)/shard_map/all_gather | solution.py:36
  88.5 3.6 fusion.56
  92.1 73.4 %all-gather.13.cloned.1.call-done = bf16[1,2048,1024]{2,1,0:T(8,128)(2,1)} async-done(((bf16[1,128,1024]{2,1,0:T(8,128)(2,1)}), bf16[1,2048,1024]{2,1,0:T(8,128)(2,1)}) %all-gather.13.cloned.1.call-update) | async-done | bytes 4194320 | tf_op jit(solution)/shard_map/all_gather | solution.py:31
  165.4 3.5 fusion.53
  169.0 3.4 collective-permute-start
  172.4 1.9 collective-permute-done
  174.4 5.8 %fusion.137 = (f32[256]{0:T(256)S(1)}, f32[256]{0:T(256)S(1)}, f32[256,1024]{1,0:T(8,128)S(1)}) fusion(f32[286,1024]{1,0:T(8,128)S(1)} %maximum_convert_fusion, f32[1024]{0:T(1024)S(1)} %bitcast.146, f32[1024]{0:T(1024)S(1)} %bitcast.147, f32[1024]{0:T(1024)S(1)} %bitcast.148, f32[1024]{0:T(1024)S(1)} %bitcast.149, f32[1024]{0:T(1024)S(1)} %bitcast.150, ...), kind=kLoop, calls=%fused_computation.185 | loop fusion | flops 16776704 | bytes 33683456 | tf_op jit(solution)/shard_map/reduce_sum | solution.py:47
  180.2 2.5 all-reduce.1
  182.7 72.8 %all-gather.17.cloned.1.call-done = bf16[1,1024,2048]{2,1,0:T(8,128)(2,1)} async-done(((bf16[1,1024,128]{2,1,0:T(8,128)(2,1)}), bf16[1,1024,2048]{2,1,0:T(8,128)(2,1)}) %all-gather.17.cloned.1.call-update) | async-done | bytes 4194320 | tf_op jit(solution)/shard_map/all_gather | solution.py:54
  255.5 4.7 fusion.12
  262.2 15.8 %all-reduce.5.cloned.1.call-done = bf16[256,2048]{1,0:T(8,128)(2,1)} async-done(((bf16[256,2048]{1,0:T(8,128)(2,1)}), bf16[256,2048]{1,0:T(8,128)(2,1)}) %all-reduce.5.cloned.1.call-update) | async-done | bytes 1048592 | tf_op jit(solution)/shard_map/psum | solution.py:56
  279.7 77.7 %all-gather.21.cloned.1.call-done = bf16[1,2048,1024]{2,1,0:T(8,128)(2,1)} async-done(((bf16[1,128,1024]{2,1,0:T(8,128)(2,1)}), bf16[1,2048,1024]{2,1,0:T(8,128)(2,1)}) %all-gather.21.cloned.1.call-update) | async-done | bytes 4194320 | tf_op jit(solution)/shard_map/all_gather | solution.py:36
  357.4 3.6 fusion.59
  361.0 73.3 %all-gather.19.cloned.1.call-done = bf16[1,2048,1024]{2,1,0:T(8,128)(2,1)} async-done(((bf16[1,128,1024]{2,1,0:T(8,128)(2,1)}), bf16[1,2048,1024]{2,1,0:T(8,128)(2,1)}) %all-gather.19.cloned.1.call-update) | async-done | bytes 4194320 | tf_op jit(solution)/shard_map/all_gather | solution.py:31
  434.3 3.5 fusion.50
  437.8 3.5 collective-permute-start.1
  443.2 5.8 %fusion.136 = (f32[256]{0:T(256)S(1)}, f32[256]{0:T(256)S(1)}, f32[256,1024]{1,0:T(8,128)S(1)}) fusion(f32[286,1024]{1,0:T(8,128)S(1)} %maximum_convert_fusion.1, f32[1024]{0:T(1024)S(1)} %bitcast.112, f32[1024]{0:T(1024)S(1)} %bitcast.113, f32[1024]{0:T(1024)S(1)} %bitcast.156, f32[1024]{0:T(1024)S(1)} %bitcast.157, f32[1024]{0:T(1024)S(1)} %bitcast.158, ...), kind=kLoop, calls=%fused_computation.184 | loop fusion | flops 16776704 | bytes 33683456 | tf_op jit(solution)/shard_map/reduce_sum | solution.py:47
  449.1 2.5 all-reduce
  451.5 72.8 %all-gather.23.cloned.1.call-done = bf16[1,1024,2048]{2,1,0:T(8,128)(2,1)} async-done(((bf16[1,1024,128]{2,1,0:T(8,128)(2,1)}), bf16[1,1024,2048]{2,1,0:T(8,128)(2,1)}) %all-gather.23.cloned.1.call-update) | async-done | bytes 4194320 | tf_op jit(solution)/shard_map/all_gather | solution.py:54
  524.3 4.7 fusion.15
  529.0 17.8 %all-reduce.7.cloned.1.call-done = bf16[256,2048]{1,0:T(8,128)(2,1)} async-done(((bf16[256,2048]{1,0:T(8,128)(2,1)}), bf16[256,2048]{1,0:T(8,128)(2,1)}) %all-reduce.7.cloned.1.call-update) | async-done | bytes 1048592 | tf_op jit(solution)/shard_map/psum | solution.py:56
  546.8 2.5 fusion.25
  (44 shorter events, 7.2 us)
Async XLA Ops:
  6.5 4.1 copy-start.1
  6.5 5.0 copy-start
  6.5 81.9 %all-gather.15.cloned.1.call-start = ((), (), s32[]{:S(2)}) async-start(), calls=%async_computation.3 | async-start | bytes 4456448 | tf_op jit(solution)/shard_map/all_gather | solution.py:36
  8.5 3.3 copy-start.2
  8.5 3.5 copy-start.3
  8.6 156.9 %all-gather.13.cloned.1.call-start = ((), (), s32[]{:S(2)}) async-start(), calls=%async_computation.2 | async-start | bytes 4456448 | tf_op jit(solution)/shard_map/all_gather | solution.py:31
  10.6 244.9 %all-gather.17.cloned.1.call-start = ((), (), s32[]{:S(2)}) async-start(), calls=%async_computation.4 | async-start | bytes 4456448 | tf_op jit(solution)/shard_map/all_gather | solution.py:54
  11.5 266.5 %all-reduce.5.cloned.1.call-start = ((), (), s32[]{:S(2)}) async-start(), calls=%async_computation | async-start | bytes 2097152 | tf_op jit(solution)/shard_map/psum | solution.py:56
  92.0 80.3 %copy-start.4 = (f32[2,1024]{1,0:T(2,128)S(1)}, f32[2,1024]{1,0:T(2,128)}, u32[]{:S(2)}) copy-start(f32[2,1024]{1,0:T(2,128)} %param.12) | copy-start | bytes 24580
  169.0 5.2 collective-permute-start
  260.2 97.2 %all-gather.21.cloned.1.call-start = ((), (), s32[]{:S(2)}) async-start(), calls=%async_computation.6 | async-start | bytes 4456448 | tf_op jit(solution)/shard_map/all_gather | solution.py:36
  260.8 173.5 %all-gather.19.cloned.1.call-start = ((), (), s32[]{:S(2)}) async-start(), calls=%async_computation.5 | async-start | bytes 4456448 | tf_op jit(solution)/shard_map/all_gather | solution.py:31
  261.4 262.9 %all-gather.23.cloned.1.call-start = ((), (), s32[]{:S(2)}) async-start(), calls=%async_computation.7 | async-start | bytes 4456448 | tf_op jit(solution)/shard_map/all_gather | solution.py:54
  262.1 284.6 %all-reduce.7.cloned.1.call-start = ((), (), s32[]{:S(2)}) async-start(), calls=%async_computation.1 | async-start | bytes 2097152 | tf_op jit(solution)/shard_map/psum | solution.py:56
  437.8 5.3 collective-permute-start.1
Sparse Core Ops, SparseCore 0:
  10.1 78.3 all-gather.14
  91.2 74.1 all-gather.12
  168.2 87.3 all-gather.16
  260.3 17.5 all-reduce.4
  280.6 76.7 all-gather.20
  360.0 74.1 all-gather.18
  437.0 87.3 all-gather.22
  529.1 17.5 all-reduce.6
where the time goes:
time: 557 us; the launch traced here: 556 us
  waiting for transfers between devices  485 us (87%)
  matrix products  23.6 us (4%)
  other arithmetic  16.5 us (3%)
  between operations  13.7 us (2%)
  starting transfers between devices  7.18 us (1%)
    all_gather x2, waiting for transfers between devices, body(): lax.all_gather(gate_weight[layer], 'sp', axis=0, tiled=True)  154 us
    all_gather x2, waiting for transfers between devices, body(): lax.all_gather(value_weight[layer], 'sp', axis=0, tiled=True)  147 us
    all_gather x2, waiting for transfers between devices, body(): whole_out = lax.all_gather(out_weight[layer], 'sp', axis=1, tiled=True)  146 us
    psum x2, waiting for transfers between devices, body(): summed = lax.psum(terms.astype(jnp.bfloat16), 'tp').astype(jnp.float32)  33.6 us
    reduce_sum x2, other arithmetic, body(): jnp.sum(filtered, axis=1)  11.6 us
  transfers between devices with their start and end apart: 10, of which 10 were waited for; matrix products, arithmetic and copies ran while one was open for 6% of the time, Pallas kernels for 0%

commit v1 on v0

--- a/solution.py
+++ b/solution.py
@@ -51,7 +51,14 @@
         activated = jax.nn.silu(
             (filtered - mean_value) * lax.rsqrt(variance + epsilon) * channel_gain[layer]
         ).astype(jnp.bfloat16)
-        whole_out = lax.all_gather(out_weight[layer], "sp", axis=1, tiled=True)
+        ring = [out_weight[layer]]
+        for hop in range(15):
+            ring.append(lax.ppermute(ring[-1], "sp", [(dev, (dev + 1) % 16) for dev in range(16)]))
+        whole_out = jnp.roll(
+            jnp.concatenate(ring[::-1], axis=1),
+            (lax.axis_index("sp") + 1) * ring[0].shape[1],
+            axis=1,
+        )
         terms = jnp.dot(activated, whole_out, preferred_element_type=jnp.float32)
         summed = lax.psum(terms.astype(jnp.bfloat16), "tp").astype(jnp.float32)
         stream = (wide + summed).astype(jnp.bfloat16)

time: 557 us -> 537 us (0.964)
  waiting for transfers between devices: 485 us -> 423 us
  local copies, waits for them, and re-layouts: 5.06 us -> 40.7 us
    ppermute x0 -> x30, waiting for transfers between devices: none -> 232 us  [body(): lax.ppermute(ring[-1], 'sp', [(dev, (dev + 1) % 16) for dev in range(16)])]
    all_gather x2 -> x0, waiting for transfers between devices: 146 us -> none  [body(): whole_out = lax.all_gather(out_weight[layer], 'sp', axis=1, tiled=True)]
    all_gather x2, waiting for transfers between devices: 154 us -> 77.7 us  [body(): lax.all_gather(gate_weight[layer], 'sp', axis=0, tiled=True)]
    all_gather x2, waiting for transfers between devices: 147 us -> 73.3 us  [body(): lax.all_gather(value_weight[layer], 'sp', axis=0, tiled=True)]
    unnamed x10 -> x112, local copies, waits for them, and re-layouts: 0.02 us -> 27.7 us
  transfers between devices with their start and end apart: 10 -> 38, of which waited for: 10 -> 35; matrix products, arithmetic and copies ran while one was open for 6% -> 8% of each run, Pallas kernels for 0% -> 0%
where the time goes in v1:
time: 537 us; the launch traced here: 536 us
  waiting for transfers between devices  423 us (79%)
  local copies, waits for them, and re-layouts  40.7 us (8%)
  matrix products  26.6 us (5%)
  other arithmetic  17.1 us (3%)
  between operations  14 us (3%)
  starting transfers between devices  9.48 us (2%)
    ppermute x30, waiting for transfers between devices, body(): lax.ppermute(ring[-1], 'sp', [(dev, (dev + 1) % 16) for dev in range(16)])  232 us
    all_gather x2, waiting for transfers between devices, body(): lax.all_gather(gate_weight[layer], 'sp', axis=0, tiled=True)  77.7 us
    all_gather x2, waiting for transfers between devices, body(): lax.all_gather(value_weight[layer], 'sp', axis=0, tiled=True)  73.3 us
    psum x2, waiting for transfers between devices, body(): summed = lax.psum(terms.astype(jnp.bfloat16), 'tp').astype(jnp.float32)  36.6 us
    unnamed x112, local copies, waits for them, and re-layouts  27.7 us
    reduce_sum x2, other arithmetic, body(): jnp.sum(filtered, axis=1)  11.6 us
    dot_general x2, matrix products, body(): terms = jnp.dot(activated, whole_out, preferred_element_type=jnp.float32)  11.2 us
  transfers between devices with their start and end apart: 38, of which 35 were waited for; matrix products, arithmetic and copies ran while one was open for 8% of the time, Pallas kernels for 0%

profile of v1, /device:TPU:0, one launch (start us, length us, event | category | flops | bytes accessed | tf_op | source)
XLA Modules:
  0.0 536.0 jit_solution(12080689881736592956)
XLA Ops:
  14.2 9.7 %collective-permute-done.17 = bf16[1024,128]{1,0:T(8,128)(2,1)S(1)} collective-permute-done((bf16[1024,128]{1,0:T(8,128)(2,1)S(1)}, bf16[1024,128]{1,0:T(8,128)(2,1)S(1)}, u32[]{:S(2)}, u32[]{:S(2)}) %collective-permute-start.17) | collective-permute-done | bytes 262176 | tf_op jit(solution)/shard_map/ppermute | solution.py:56
  23.8 6.5 %collective-permute-done.1 = bf16[1024,128]{1,0:T(8,128)(2,1)S(1)} collective-permute-done((bf16[1024,128]{1,0:T(8,128)(2,1)S(1)}, bf16[1024,128]{1,0:T(8,128)(2,1)S(1)}, u32[]{:S(2)}, u32[]{:S(2)}) %collective-permute-start.1) | collective-permute-done | bytes 262176 | tf_op jit(solution)/shard_map/ppermute | solution.py:56
  30.4 10.2 %collective-permute-done.18 = bf16[1024,128]{1,0:T(8,128)(2,1)S(1)} collective-permute-done((bf16[1024,128]{1,0:T(8,128)(2,1)S(1)}, bf16[1024,128]{1,0:T(8,128)(2,1)S(1)}, u32[]{:S(2)}, u32[]{:S(2)}) %collective-permute-start.18) | collective-permute-done | bytes 262176 | tf_op jit(solution)/shard_map/ppermute | solution.py:56
  63.2 6.3 %collective-permute-done.4 = bf16[1024,128]{1,0:T(8,128)(2,1)S(1)} collective-permute-done((bf16[1024,128]{1,0:T(8,128)(2,1)S(1)}, bf16[1024,128]{1,0:T(8,128)(2,1)S(1)}, u32[]{:S(2)}, u32[]{:S(2)}) %collective-permute-start.4) | collective-permute-done | bytes 262176 | tf_op jit(solution)/shard_map/ppermute | solution.py:56
  69.5 9.4 %collective-permute-done.21 = bf16[1024,128]{1,0:T(8,128)(2,1)S(1)} collective-permute-done((bf16[1024,128]{1,0:T(8,128)(2,1)S(1)}, bf16[1024,128]{1,0:T(8,128)(2,1)S(1)}, u32[]{:S(2)}, u32[]{:S(2)}) %collective-permute-start.21) | collective-permute-done | bytes 262176 | tf_op jit(solution)/shard_map/ppermute | solution.py:56
  78.9 10.2 %collective-permute-done.5 = bf16[1024,128]{1,0:T(8,128)(2,1)S(1)} collective-permute-done((bf16[1024,128]{1,0:T(8,128)(2,1)S(1)}, bf16[1024,128]{1,0:T(8,128)(2,1)S(1)}, u32[]{:S(2)}, u32[]{:S(2)}) %collective-permute-start.5) | collective-permute-done | bytes 262176 | tf_op jit(solution)/shard_map/ppermute | solution.py:56
  89.1 9.3 %collective-permute-done.22 = bf16[1024,128]{1,0:T(8,128)(2,1)S(1)} collective-permute-done((bf16[1024,128]{1,0:T(8,128)(2,1)S(1)}, bf16[1024,128]{1,0:T(8,128)(2,1)S(1)}, u32[]{:S(2)}, u32[]{:S(2)}) %collective-permute-start.22) | collective-permute-done | bytes 262176 | tf_op jit(solution)/shard_map/ppermute | solution.py:56
  104.7 11.5 %collective-permute-done.23 = bf16[1024,128]{1,0:T(8,128)(2,1)S(1)} collective-permute-done((bf16[1024,128]{1,0:T(8,128)(2,1)S(1)}, bf16[1024,128]{1,0:T(8,128)(2,1)S(1)}, u32[]{:S(2)}, u32[]{:S(2)}) %collective-permute-start.23) | collective-permute-done | bytes 262176 | tf_op jit(solution)/shard_map/ppermute | solution.py:56
  116.3 11.2 %collective-permute-done.7 = bf16[1024,128]{1,0:T(8,128)(2,1)S(1)} collective-permute-done((bf16[1024,128]{1,0:T(8,128)(2,1)S(1)}, bf16[1024,128]{1,0:T(8,128)(2,1)S(1)}, u32[]{:S(2)}, u32[]{:S(2)}) %collective-permute-start.7) | collective-permute-done | bytes 262176 | tf_op jit(solution)/shard_map/ppermute | solution.py:56
  128.2 9.7 %collective-permute-done.24 = bf16[1024,128]{1,0:T(8,128)(2,1)S(1)} collective-permute-done((bf16[1024,128]{1,0:T(8,128)(2,1)S(1)}, bf16[1024,128]{1,0:T(8,128)(2,1)S(1)}, u32[]{:S(2)}, u32[]{:S(2)}) %collective-permute-start.24) | collective-permute-done | bytes 262176 | tf_op jit(solution)/shard_map/ppermute | solution.py:56
  137.9 11.2 %collective-permute-done.8 = bf16[1024,128]{1,0:T(8,128)(2,1)S(1)} collective-permute-done((bf16[1024,128]{1,0:T(8,128)(2,1)S(1)}, bf16[1024,128]{1,0:T(8,128)(2,1)S(1)}, u32[]{:S(2)}, u32[]{:S(2)}) %collective-permute-start.8) | collective-permute-done | bytes 262176 | tf_op jit(solution)/shard_map/ppermute | solution.py:56
  155.9 6.6 %collective-permute-done.9 = bf16[1024,128]{1,0:T(8,128)(2,1)S(1)} collective-permute-done((bf16[1024,128]{1,0:T(8,128)(2,1)S(1)}, bf16[1024,128]{1,0:T(8,128)(2,1)S(1)}, u32[]{:S(2)}, u32[]{:S(2)}) %collective-permute-start.9) | collective-permute-done | bytes 262176 | tf_op jit(solution)/shard_map/ppermute | solution.py:56
  163.3 7.5 %collective-permute-done.26 = bf16[1024,128]{1,0:T(8,128)(2,1)S(1)} collective-permute-done((bf16[1024,128]{1,0:T(8,128)(2,1)S(1)}, bf16[1024,128]{1,0:T(8,128)(2,1)S(1)}, u32[]{:S(2)}, u32[]{:S(2)}) %collective-permute-start.26) | collective-permute-done | bytes 262176 | tf_op jit(solution)/shard_map/ppermute | solution.py:56
  170.7 9.2 %collective-permute-done.10 = bf16[1024,128]{1,0:T(8,128)(2,1)S(1)} collective-permute-done((bf16[1024,128]{1,0:T(8,128)(2,1)S(1)}, bf16[1024,128]{1,0:T(8,128)(2,1)S(1)}, u32[]{:S(2)}, u32[]{:S(2)}) %collective-permute-start.10) | collective-permute-done | bytes 262176 | tf_op jit(solution)/shard_map/ppermute | solution.py:56
  191.7 11.2 %collective-permute-done.28 = bf16[1024,128]{1,0:T(8,128)(2,1)S(1)} collective-permute-done((bf16[1024,128]{1,0:T(8,128)(2,1)S(1)}, bf16[1024,128]{1,0:T(8,128)(2,1)S(1)}, u32[]{:S(2)}, u32[]{:S(2)}) %collective-permute-start.28) | collective-permute-done | bytes 262176 | tf_op jit(solution)/shard_map/ppermute | solution.py:56
  205.0 7.4 %collective-permute-done.12 = bf16[1024,128]{1,0:T(8,128)(2,1)S(1)} collective-permute-done((bf16[1024,128]{1,0:T(8,128)(2,1)S(1)}, bf16[1024,128]{1,0:T(8,128)(2,1)S(1)}, u32[]{:S(2)}, u32[]{:S(2)}) %collective-permute-start.12) | collective-permute-done | bytes 262176 | tf_op jit(solution)/shard_map/ppermute | solution.py:56
  213.1 7.3 %collective-permute-done.29 = bf16[1024,128]{1,0:T(8,128)(2,1)S(1)} collective-permute-done((bf16[1024,128]{1,0:T(8,128)(2,1)S(1)}, bf16[1024,128]{1,0:T(8,128)(2,1)S(1)}, u32[]{:S(2)}, u32[]{:S(2)}) %collective-permute-start.29) | collective-permute-done | bytes 262176 | tf_op jit(solution)/shard_map/ppermute | solution.py:56
  225.5 13.4 %collective-permute-done.30 = bf16[1024,128]{1,0:T(8,128)(2,1)} collective-permute-done((bf16[1024,128]{1,0:T(8,128)(2,1)S(1)}, bf16[1024,128]{1,0:T(8,128)(2,1)}, u32[]{:S(2)}, u32[]{:S(2)}) %collective-permute-start.30) | collective-permute-done | bytes 262176 | tf_op jit(solution)/shard_map/ppermute | solution.py:56
  241.1 9.1 %collective-permute-done.14 = bf16[1024,128]{1,0:T(8,128)(2,1)} collective-permute-done((bf16[1024,128]{1,0:T(8,128)(2,1)}, bf16[1024,128]{1,0:T(8,128)(2,1)}, u32[]{:S(2)}, u32[]{:S(2)}) %collective-permute-start.14) | collective-permute-done | bytes 262176 | tf_op jit(solution)/shard_map/ppermute | solution.py:56
  250.2 10.5 %collective-permute-done.31 = bf16[1024,128]{1,0:T(8,128)(2,1)} collective-permute-done((bf16[1024,128]{1,0:T(8,128)(2,1)}, bf16[1024,128]{1,0:T(8,128)(2,1)}, u32[]{:S(2)}, u32[]{:S(2)}) %collective-permute-start.31) | collective-permute-done | bytes 262176 | tf_op jit(solution)/shard_map/ppermute | solution.py:56
  310.8 16.6 %all-reduce.5.cloned.1.call-done = bf16[256,2048]{1,0:T(8,128)(2,1)} async-done(((bf16[256,2048]{1,0:T(8,128)(2,1)}), bf16[256,2048]{1,0:T(8,128)(2,1)}) %all-reduce.5.cloned.1.call-update) | async-done | bytes 1048592 | tf_op jit(solution)/shard_map/psum | solution.py:63
  329.2 77.7 %all-gather.15.cloned.1.call-done = bf16[1,2048,1024]{2,1,0:T(8,128)(2,1)} async-done(((bf16[1,128,1024]{2,1,0:T(8,128)(2,1)}), bf16[1,2048,1024]{2,1,0:T(8,128)(2,1)}) %all-gather.15.cloned.1.call-update) | async-done | bytes 4194320 | tf_op jit(solution)/shard_map/all_gather | solution.py:36
  410.5 73.3 %all-gather.13.cloned.1.call-done = bf16[1,2048,1024]{2,1,0:T(8,128)(2,1)} async-done(((bf16[1,128,1024]{2,1,0:T(8,128)(2,1)}), bf16[1,2048,1024]{2,1,0:T(8,128)(2,1)}) %all-gather.13.cloned.1.call-update) | async-done | bytes 4194320 | tf_op jit(solution)/shard_map/all_gather | solution.py:31
  506.6 20.0 %all-reduce.7.cloned.1.call-done = bf16[256,2048]{1,0:T(8,128)(2,1)} async-done(((bf16[256,2048]{1,0:T(8,128)(2,1)}), bf16[256,2048]{1,0:T(8,128)(2,1)}) %all-reduce.7.cloned.1.call-update) | async-done | bytes 1048592 | tf_op jit(solution)/shard_map/psum | solution.py:63
  (201 shorter events, 147.1 us)
Async XLA Ops:
  6.5 277.1 %all-gather.11.cloned.1.call-start = ((), (), s32[]{:S(2)}) async-start(), calls=%async_computation.3 | async-start | bytes 4456448 | tf_op jit(solution)/shard_map/all_gather | solution.py:36
  8.5 279.7 %all-gather.9.cloned.1.call-start = ((), (), s32[]{:S(2)}) async-start(), calls=%async_computation.2 | async-start | bytes 4456448 | tf_op jit(solution)/shard_map/all_gather | solution.py:31
  12.7 17.7 %collective-permute-start.1 = (bf16[1024,128]{1,0:T(8,128)(2,1)S(1)}, bf16[1024,128]{1,0:T(8,128)(2,1)S(1)}, u32[]{:S(2)}, u32[]{:S(2)}) collective-permute-start(bf16[1024,128]{1,0:T(8,128)(2,1)S(1)} %get-tuple-element.25), channel_id=1, source_target_pairs={{0,2},{2,4},{4,6},{6,8},{8,10},{10,12},{12,14},{14,16},{16,18},{18... | collective-permute-start | bytes 786440 | tf_op jit(solution)/shard_map/ppermute | solution.py:56
  23.8 16.7 %collective-permute-start.18 = (bf16[1024,128]{1,0:T(8,128)(2,1)S(1)}, bf16[1024,128]{1,0:T(8,128)(2,1)S(1)}, u32[]{:S(2)}, u32[]{:S(2)}) collective-permute-start(bf16[1024,128]{1,0:T(8,128)(2,1)S(1)} %collective-permute-done.17), channel_id=1, source_target_pairs={{0,2},{2,4},{4,6},{6,8},{8,10},{10,12},{12,14},{14,16},{16,18},{18... | collective-permute-start | bytes 786440 | tf_op jit(solution)/shard_map/ppermute | solution.py:56
  53.0 274.4 %all-reduce.5.cloned.1.call-start = ((), (), s32[]{:S(2)}) async-start(), calls=%async_computation | async-start | bytes 2097152 | tf_op jit(solution)/shard_map/psum | solution.py:63
  63.2 15.7 %collective-permute-start.21 = (bf16[1024,128]{1,0:T(8,128)(2,1)S(1)}, bf16[1024,128]{1,0:T(8,128)(2,1)S(1)}, u32[]{:S(2)}, u32[]{:S(2)}) collective-permute-start(bf16[1024,128]{1,0:T(8,128)(2,1)S(1)} %collective-permute-done.20), channel_id=1, source_target_pairs={{0,2},{2,4},{4,6},{6,8},{8,10},{10,12},{12,14},{14,16},{16,18},{18... | collective-permute-start | bytes 786440 | tf_op jit(solution)/shard_map/ppermute | solution.py:56
  69.5 19.6 %collective-permute-start.5 = (bf16[1024,128]{1,0:T(8,128)(2,1)S(1)}, bf16[1024,128]{1,0:T(8,128)(2,1)S(1)}, u32[]{:S(2)}, u32[]{:S(2)}) collective-permute-start(bf16[1024,128]{1,0:T(8,128)(2,1)S(1)} %collective-permute-done.4), channel_id=1, source_target_pairs={{0,2},{2,4},{4,6},{6,8},{8,10},{10,12},{12,14},{14,16},{16,18},{18... | collective-permute-start | bytes 786440 | tf_op jit(solution)/shard_map/ppermute | solution.py:56
  78.9 19.5 %collective-permute-start.22 = (bf16[1024,128]{1,0:T(8,128)(2,1)S(1)}, bf16[1024,128]{1,0:T(8,128)(2,1)S(1)}, u32[]{:S(2)}, u32[]{:S(2)}) collective-permute-start(bf16[1024,128]{1,0:T(8,128)(2,1)S(1)} %collective-permute-done.21), channel_id=1, source_target_pairs={{0,2},{2,4},{4,6},{6,8},{8,10},{10,12},{12,14},{14,16},{16,18},{18... | collective-permute-start | bytes 786440 | tf_op jit(solution)/shard_map/ppermute | solution.py:56
  98.4 17.9 %collective-permute-start.23 = (bf16[1024,128]{1,0:T(8,128)(2,1)S(1)}, bf16[1024,128]{1,0:T(8,128)(2,1)S(1)}, u32[]{:S(2)}, u32[]{:S(2)}) collective-permute-start(bf16[1024,128]{1,0:T(8,128)(2,1)S(1)} %collective-permute-done.22), channel_id=1, source_target_pairs={{0,2},{2,4},{4,6},{6,8},{8,10},{10,12},{12,14},{14,16},{16,18},{18... | collective-permute-start | bytes 786440 | tf_op jit(solution)/shard_map/ppermute | solution.py:56
  104.7 22.8 %collective-permute-start.7 = (bf16[1024,128]{1,0:T(8,128)(2,1)S(1)}, bf16[1024,128]{1,0:T(8,128)(2,1)S(1)}, u32[]{:S(2)}, u32[]{:S(2)}) collective-permute-start(bf16[1024,128]{1,0:T(8,128)(2,1)S(1)} %collective-permute-done.6), channel_id=1, source_target_pairs={{0,2},{2,4},{4,6},{6,8},{8,10},{10,12},{12,14},{14,16},{16,18},{18... | collective-permute-start | bytes 786440 | tf_op jit(solution)/shard_map/ppermute | solution.py:56
  116.3 21.6 %collective-permute-start.24 = (bf16[1024,128]{1,0:T(8,128)(2,1)S(1)}, bf16[1024,128]{1,0:T(8,128)(2,1)S(1)}, u32[]{:S(2)}, u32[]{:S(2)}) collective-permute-start(bf16[1024,128]{1,0:T(8,128)(2,1)S(1)} %collective-permute-done.23), channel_id=1, source_target_pairs={{0,2},{2,4},{4,6},{6,8},{8,10},{10,12},{12,14},{14,16},{16,18},{18... | collective-permute-start | bytes 786440 | tf_op jit(solution)/shard_map/ppermute | solution.py:56
  128.2 20.9 %collective-permute-start.8 = (bf16[1024,128]{1,0:T(8,128)(2,1)S(1)}, bf16[1024,128]{1,0:T(8,128)(2,1)S(1)}, u32[]{:S(2)}, u32[]{:S(2)}) collective-permute-start(bf16[1024,128]{1,0:T(8,128)(2,1)S(1)} %collective-permute-done.7), channel_id=1, source_target_pairs={{0,2},{2,4},{4,6},{6,8},{8,10},{10,12},{12,14},{14,16},{16,18},{18... | collective-permute-start | bytes 786440 | tf_op jit(solution)/shard_map/ppermute | solution.py:56
  137.9 18.0 %collective-permute-start.25 = (bf16[1024,128]{1,0:T(8,128)(2,1)S(1)}, bf16[1024,128]{1,0:T(8,128)(2,1)S(1)}, u32[]{:S(2)}, u32[]{:S(2)}) collective-permute-start(bf16[1024,128]{1,0:T(8,128)(2,1)S(1)} %collective-permute-done.24), channel_id=1, source_target_pairs={{0,2},{2,4},{4,6},{6,8},{8,10},{10,12},{12,14},{14,16},{16,18},{18... | collective-permute-start | bytes 786440 | tf_op jit(solution)/shard_map/ppermute | solution.py:56
  162.6 17.3 %collective-permute-start.10 = (bf16[1024,128]{1,0:T(8,128)(2,1)S(1)}, bf16[1024,128]{1,0:T(8,128)(2,1)S(1)}, u32[]{:S(2)}, u32[]{:S(2)}) collective-permute-start(bf16[1024,128]{1,0:T(8,128)(2,1)S(1)} %collective-permute-done.9), channel_id=1, source_target_pairs={{0,2},{2,4},{4,6},{6,8},{8,10},{10,12},{12,14},{14,16},{16,18},{18... | collective-permute-start | bytes 786440 | tf_op jit(solution)/shard_map/ppermute | solution.py:56
  185.1 17.8 %collective-permute-start.28 = (bf16[1024,128]{1,0:T(8,128)(2,1)S(1)}, bf16[1024,128]{1,0:T(8,128)(2,1)S(1)}, u32[]{:S(2)}, u32[]{:S(2)}) collective-permute-start(bf16[1024,128]{1,0:T(8,128)(2,1)S(1)} %collective-permute-done.27), channel_id=1, source_target_pairs={{0,2},{2,4},{4,6},{6,8},{8,10},{10,12},{12,14},{14,16},{16,18},{18... | collective-permute-start | bytes 786440 | tf_op jit(solution)/shard_map/ppermute | solution.py:56
  191.7 20.7 %collective-permute-start.12 = (bf16[1024,128]{1,0:T(8,128)(2,1)S(1)}, bf16[1024,128]{1,0:T(8,128)(2,1)S(1)}, u32[]{:S(2)}, u32[]{:S(2)}) collective-permute-start(bf16[1024,128]{1,0:T(8,128)(2,1)S(1)} %collective-permute-done.11), channel_id=1, source_target_pairs={{0,2},{2,4},{4,6},{6,8},{8,10},{10,12},{12,14},{14,16},{16,18},{18... | collective-permute-start | bytes 786440 | tf_op jit(solution)/shard_map/ppermute | solution.py:56
  202.9 17.6 %collective-permute-start.29 = (bf16[1024,128]{1,0:T(8,128)(2,1)S(1)}, bf16[1024,128]{1,0:T(8,128)(2,1)S(1)}, u32[]{:S(2)}, u32[]{:S(2)}) collective-permute-start(bf16[1024,128]{1,0:T(8,128)(2,1)S(1)} %collective-permute-done.28), channel_id=1, source_target_pairs={{0,2},{2,4},{4,6},{6,8},{8,10},{10,12},{12,14},{14,16},{16,18},{18... | collective-permute-start | bytes 786440 | tf_op jit(solution)/shard_map/ppermute | solution.py:56
  220.4 18.5 %collective-permute-start.30 = (bf16[1024,128]{1,0:T(8,128)(2,1)S(1)}, bf16[1024,128]{1,0:T(8,128)(2,1)}, u32[]{:S(2)}, u32[]{:S(2)}) collective-permute-start(bf16[1024,128]{1,0:T(8,128)(2,1)S(1)} %collective-permute-done.29), channel_id=1, source_target_pairs={{0,2},{2,4},{4,6},{6,8},{8,10},{10,12},{12,14},{14,16},{16,18},{18... | collective-permute-start | bytes 786440 | tf_op jit(solution)/shard_map/ppermute | solution.py:56
  225.5 24.6 %collective-permute-start.14 = (bf16[1024,128]{1,0:T(8,128)(2,1)}, bf16[1024,128]{1,0:T(8,128)(2,1)}, u32[]{:S(2)}, u32[]{:S(2)}) collective-permute-start(bf16[1024,128]{1,0:T(8,128)(2,1)} %collective-permute-done.13), channel_id=1, source_target_pairs={{0,2},{2,4},{4,6},{6,8},{8,10},{10,12},{12,14},{14,16},{16,18},{18... | collective-permute-start | bytes 786440 | tf_op jit(solution)/shard_map/ppermute | solution.py:56
  238.9 21.7 %collective-permute-start.31 = (bf16[1024,128]{1,0:T(8,128)(2,1)}, bf16[1024,128]{1,0:T(8,128)(2,1)}, u32[]{:S(2)}, u32[]{:S(2)}) collective-permute-start(bf16[1024,128]{1,0:T(8,128)(2,1)} %collective-permute-done.30), channel_id=1, source_target_pairs={{0,2},{2,4},{4,6},{6,8},{8,10},{10,12},{12,14},{14,16},{16,18},{18... | collective-permute-start | bytes 786440 | tf_op jit(solution)/shard_map/ppermute | solution.py:56
  250.2 19.9 %collective-permute-start.15 = (bf16[1024,128]{1,0:T(8,128)(2,1)}, bf16[1024,128]{1,0:T(8,128)(2,1)S(1)}, u32[]{:S(2)}, u32[]{:S(2)}) collective-permute-start(bf16[1024,128]{1,0:T(8,128)(2,1)} %collective-permute-done.14), channel_id=1, source_target_pairs={{0,2},{2,4},{4,6},{6,8},{8,10},{10,12},{12,14},{14,16},{16,18},{18... | collective-permute-start | bytes 786440 | tf_op jit(solution)/shard_map/ppermute | solution.py:56
  309.6 97.3 %all-gather.15.cloned.1.call-start = ((), (), s32[]{:S(2)}) async-start(), calls=%async_computation.5 | async-start | bytes 4456448 | tf_op jit(solution)/shard_map/all_gather | solution.py:36
  310.2 173.5 %all-gather.13.cloned.1.call-start = ((), (), s32[]{:S(2)}) async-start(), calls=%async_computation.4 | async-start | bytes 4456448 | tf_op jit(solution)/shard_map/all_gather | solution.py:31
  310.8 215.8 %all-reduce.7.cloned.1.call-start = ((), (), s32[]{:S(2)}) async-start(), calls=%async_computation.1 | async-start | bytes 2097152 | tf_op jit(solution)/shard_map/psum | solution.py:63
  (55 other events, 1047.4 us)
Sparse Core Ops, SparseCore 0:
  10.1 133.0 all-gather.10
  145.9 116.9 all-gather.8
  309.7 17.6 all-reduce.4
  330.1 76.7 all-gather.14
  409.5 74.1 all-gather.12
  506.7 19.8 all-reduce.6
